TPU v7x, 512 devices: a 4x2x32 block of a 4x8x32 slice. The times are simulated.
512 devices in a mesh: grp: 2 (over y), ep: 64 (over z, core), tp: 4 (over x).
Axes of the slice: x: 4, y: 2, z: 32, core: 2. Of those that a mesh axis runs over, the one named last changes fastest.
The devices are a block of a 4x8x32 slice.
Arguments:
- tokens: bfloat16 [49152, 2048], P(('grp', 'ep'), 'tp'), parts along dimension 0
- group_choice: int32 [49152], P(('grp', 'ep')), parts along dimension 0, may hold values from 0 to 7, as said below
- expert_choice: int32 [49152, 2], P(('grp', 'ep')), parts along dimension 0, may hold values from 0 to 7, as said below
- group_weight: float32 [49152], P(('grp', 'ep')), parts along dimension 0, may hold values from 0.3 to 1
- expert_weight: float32 [49152, 2], P(('grp', 'ep')), parts along dimension 0, may hold values from 0.1 to 1
- norm_gain: float32 [2048], replicated, may hold values from 0.1 to 1.9
- w_gate: bfloat16 [64, 2048, 1024], P('ep', None, 'tp'), may hold values from -0.125 to 0.125
- w_up: bfloat16 [64, 2048, 1024], P('ep', None, 'tp'), may hold values from -0.125 to 0.125
- w_down: bfloat16 [64, 1024, 2048], P('ep', None, 'tp'), may hold values from -0.1875 to 0.1875
Outputs:
- moe_out: bfloat16 [49152, 2048], P(('grp', 'ep'), 'tp'), parts along dimension 0
There are 2 independent parts, one for each index of `grp`. A program takes and returns all parts, laid end to end along the dimension named above; an argument that names none is the same for every part. Nothing has to cross between parts.
Inputs may be any that keep to these rules, and one draw needn't show every extreme that they name: `group_choice`: group of each token, 0 to 7; within each aligned block of 384 tokens (the tokens of one index of ep) every group is chosen by the same number of tokens. `expert_choice`: a token's two entries differ; within each aligned block of 384 tokens no expert (group with entry) is named by more than 18 tokens, and in every block one expert of each group, the same one in all blocks, is named by exactly 18 tokens.
All inputs are finite; a program needn't handle non-finite values.
Results may differ from a plain program's by a relative error of at most 0.0071.
Values may be sent and summed in bfloat16 or wider, within the bound.
A program may use at most 64 MiB of HBM per device.

v0:
```python
import jax
import jax.numpy as jnp
from jax import lax
from jax.sharding import Mesh
from jax.sharding import PartitionSpec as P

EP = ("ep_0", "ep_1")
GRP_EP = ("grp", "ep_0", "ep_1")


def copy_for_each(array, axis):
    length = lax.axis_size(axis)
    return lax.all_to_all(
        jnp.broadcast_to(array[None], (length, *array.shape)), axis, 0, 0, tiled=True
    )


def laid_out(blocks, dim):
    dims = list(blocks.shape[1:])
    dims[dim] *= blocks.shape[0]
    return jnp.moveaxis(blocks, 0, dim).reshape(dims)


def collect(array, axis, dim):
    blocks = copy_for_each(array, axis)
    return laid_out(blocks, dim)


def over_copies(array, axis):
    everything = copy_for_each(array, axis)
    return jnp.sum(everything, axis=0)


def cut_along(array, dim, length):
    dims = array.shape
    blocks = array.reshape(*dims[:dim], length, dims[dim] // length, *dims[dim + 1 :])
    return jnp.moveaxis(blocks, dim, 0)


def moved_by_axis(blocks, axes, turns):
    dims = [lax.axis_size(a) for a in axes]
    blocks = blocks.reshape(*dims, *blocks.shape[1:])
    for k in turns:
        blocks = lax.all_to_all(blocks, axes[k], split_axis=k, concat_axis=k, tiled=True)
    return blocks.reshape(-1, *blocks.shape[len(axes) :])


def exchange_by_chip(array, groups, turns, split_dim, concat_dim):
    length = lax.axis_size(groups[0]) * lax.axis_size(groups[1])
    blocks = cut_along(array, split_dim, length)
    return laid_out(moved_by_axis(blocks, groups, turns), concat_dim)


def finish_rows(gate_sum, up_sum, w_down):
    hidden = (jax.nn.silu(gate_sum) * up_sum).astype(jnp.bfloat16)
    whole_hidden = collect(hidden, "tp", 3)
    summed = jnp.einsum("sxcf,xfd->sxcd", whole_hidden, w_down, preferred_element_type=jnp.float32)
    return summed.astype(jnp.bfloat16)


def body(
    tokens,
    group_choice,
    expert_choice,
    group_weight,
    expert_weight,
    norm_gain,
    w_gate,
    w_up,
    w_down,
):
    tok_rows = tokens.shape[0]
    ep_count = lax.axis_size(EP)
    exp_local = w_gate.shape[0]
    experts_all = ep_count * exp_local
    group_size = min(8, experts_all // 2)
    group_count = experts_all // group_size
    mean_load = 2 * tok_rows // experts_all
    capacity = mean_load + min(mean_load // 2, tok_rows // group_count - mean_load)
    model_width = norm_gain.shape[0]
    expert_ids = group_choice[:, None] * group_size + expert_choice
    mixing = group_weight[:, None] * expert_weight / jnp.sum(expert_weight, -1, keepdims=True)
    flat_ids = expert_ids.reshape(-1)
    marks = (flat_ids[:, None] == jnp.arange(experts_all, dtype=jnp.int32)[None, :]).astype(
        jnp.int32
    )
    earlier = jnp.cumsum(marks, 0) - marks
    seat_index = jnp.sum(earlier * marks, 1)
    targets = (flat_ids * capacity + seat_index).reshape(tok_rows, 2)
    places = jnp.arange(experts_all * capacity, dtype=jnp.int32)
    dispatch = (
        (places[:, None] == targets[None, :, 0]) | (places[:, None] == targets[None, :, 1])
    ).astype(jnp.bfloat16)
    values = tokens.astype(jnp.float32)
    own_squares = jnp.sum(values * values, -1)
    all_squares = over_copies(own_squares, "tp")
    inv_rms = lax.rsqrt(all_squares / model_width + 1e-06)
    piece_width = tokens.shape[1]
    gain_piece = lax.dynamic_slice_in_dim(
        norm_gain, lax.axis_index("tp") * piece_width, piece_width, 0
    )
    normed = (values * inv_rms[:, None] * gain_piece[None, :]).astype(jnp.bfloat16)
    buffer = jnp.dot(dispatch, normed, preferred_element_type=jnp.float32).astype(jnp.bfloat16)
    buffer = buffer.reshape(ep_count, exp_local, capacity, piece_width)
    piece = lax.all_gather(
        lax.all_to_all(buffer, EP, split_axis=0, concat_axis=0, tiled=True),
        "tp",
        axis=3,
        tiled=True,
    )
    gate_next = jnp.einsum("sxcd,xdf->sxcf", piece, w_gate, preferred_element_type=jnp.float32)
    up_next = jnp.einsum("sxcd,xdf->sxcf", piece, w_up, preferred_element_type=jnp.float32)
    results = finish_rows(gate_next, up_next, w_down)
    returned = exchange_by_chip(results, ("ep_0", "ep_1"), (1, 0), 0, 0)
    returned = returned.reshape(experts_all * capacity, returned.shape[3])
    combined = jnp.zeros((tok_rows, returned.shape[1]), jnp.float32)
    for choice_index in range(2):
        picker = (targets[:, choice_index : choice_index + 1] == places[None, :]).astype(
            jnp.bfloat16
        )
        picked = jnp.dot(picker, returned, preferred_element_type=jnp.float32)
        combined = combined + mixing[:, choice_index : choice_index + 1] * picked
    return combined.astype(jnp.bfloat16)


def solution(mesh):
    split = Mesh(
        mesh.devices.reshape(mesh.shape["grp"], 32, 2, mesh.shape["tp"]),
        ("grp", "ep_0", "ep_1", "tp"),
    )
    placed = (
        P(GRP_EP, "tp"),
        P(GRP_EP),
        P(GRP_EP, None),
        P(GRP_EP),
        P(GRP_EP, None),
        P(),
        P(EP, None, "tp"),
        P(EP, None, "tp"),
        P(EP, None, "tp"),
    )
    return jax.shard_map(
        body, mesh=split, in_specs=placed, out_specs=P(GRP_EP, "tp"), check_vma=False
    )
```

profile of v0, /device:TPU:33, one launch (start us, length us, event | category | flops | bytes accessed | tf_op | source)
XLA Modules:
  0.0 482.4 jit_solution(356377158643691526)
XLA Ops:
  6.6 1.2 fusion.35
  7.8 0.6 broadcast_in_dim.6
  8.4 5.1 %all-to-all-start = ((f32[4,1,384]{2,1,0:T(1,128)}), f32[4,1,384]{2,1,0:T(1,128)S(1)}, u32[]{:S(2)}, u32[]{:S(2)}) async-start(f32[4,1,384]{2,1,0:T(1,128)} %broadcast_in_dim.6), calls=%async_computation | async-start | bytes 12288 | tf_op jit(solution)/shard_map/all_to_all | solution.py:13
  13.5 0.8 copy.35
  14.3 0.7 broadcast_multiply_fusion
  15.5 1.8 reduce-window.6
  17.3 0.3 slice_reduce_fusion.2
  17.7 0.2 reduce_sum.40
  18.0 0.3 slice_reduce_fusion.1
  18.3 0.8 dynamic_slice.3
  19.1 1.9 convolution_convert_fusion
  21.0 2.2 reshape.67
  23.2 199.5 %all_to_all.26 = bf16[64,1,18,512]{3,2,1,0:T(8,128)(2,1)S(1)} all-to-all(bf16[64,1,18,512]{3,2,1,0:T(8,128)(2,1)S(1)} %bitcast.87), channel_id=1, replica_groups=mesh['grp'=2,'ep_0'=32,'ep_1'=2,'tp'=4] {'ep_0','ep_1'}, dimensions={0} | all-to-all | bytes 2359296 | tf_op jit(solution)/shard_map/all_to_all | solution.py:106
  222.7 1.4 copy.39
  224.2 52.9 %all-gather.2.cloned.1.call-done = bf16[64,1,18,2048]{3,0,2,1:T(8,128)(2,1)} async-done(((bf16[64,1,18,512]{3,0,2,1:T(8,128)(2,1)}), bf16[64,1,18,2048]{3,0,2,1:T(8,128)(2,1)}) %all-gather.2.cloned.1.call-update) | async-done | bytes 4718608 | tf_op jit(solution)/shard_map/all_gather | solution.py:105
  277.1 3.9 fusion.9
  281.0 1.5 fusion.25
  282.5 0.3 broadcast_in_dim.8
  282.8 31.1 %all_to_all.27 = bf16[4,64,1,18,256]{4,1,3,2,0:T(8,128)(2,1)S(1)} all-to-all(bf16[4,64,1,18,256]{4,1,3,2,0:T(8,128)(2,1)S(1)} %broadcast_in_dim.8), channel_id=1, replica_groups=mesh['grp'=2,'ep_0'=32,'ep_1'=2,'tp'=4] {'tp'}, dimensions={0} | all-to-all | bytes 4718592 | tf_op jit(solution)/shard_map/all_to_all | solution.py:13
  313.9 2.0 copy.40
  315.9 2.9 reshape.71
  318.8 3.0 fusion.8
  321.9 0.5 reshape_reshape.3
  322.4 0.2 copy.41
  322.6 6.3 %all_to_all.28 = bf16[32,2,1,1,18,512]{5,0,4,3,2,1:T(8,128)(2,1)S(1)} all-to-all(bf16[32,2,1,1,18,512]{5,0,4,3,2,1:T(8,128)(2,1)S(1)} %copy.41), channel_id=1, replica_groups=mesh['grp'=2,'ep_0'=32,'ep_1'=2,'tp'=4] {'ep_1'}, dimensions={1} | all-to-all | bytes 2359296 | tf_op jit(solution)/shard_map/all_to_all | solution.py:44
  328.9 2.3 copy.42
  331.2 23.3 %all-to-all-start.4 = ((bf16[32,2,1,1,18,512]{5,1,4,3,2,0:T(2,128)(2,1)}), bf16[32,2,1,1,18,512]{5,1,4,3,2,0:T(2,128)(2,1)}, u32[]{:S(2)}, u32[]{:S(2)}) async-start(bf16[32,2,1,1,18,512]{5,1,4,3,2,0:T(2,128)(2,1)} %copy.42), calls=%async_computation.4 | async-start | bytes 2359296 | tf_op jit(solution)/shard_map/all_to_all | solution.py:44
  354.6 114.5 %all-to-all-done.4 = bf16[32,2,1,1,18,512]{5,1,4,3,2,0:T(2,128)(2,1)} async-done(((bf16[32,2,1,1,18,512]{5,1,4,3,2,0:T(2,128)(2,1)}), bf16[32,2,1,1,18,512]{5,1,4,3,2,0:T(2,128)(2,1)}, u32[]{:S(2)}, u32[]{:S(2)}) %all-to-all-start.4) | async-done | bytes 1179680 | tf_op jit(solution)/shard_map/all_to_all | solution.py:44
  469.1 1.6 copy.43
  470.7 1.2 reshape_reshape_reshape.3
  472.0 2.1 fusion.23
  474.0 1.5 fusion.24
  (31 shorter events, 0.9 us)
Async XLA Ops:
  6.5 312.3 %copy-start = (bf16[1,1024,512]{2,1,0:T(8,128)(2,1)S(1)}, bf16[1,1024,512]{2,1,0:T(8,128)(2,1)}, u32[]{:S(2)}) copy-start(bf16[1,1024,512]{2,1,0:T(8,128)(2,1)} %param.17) | copy-start | bytes 3145732
  8.4 10.6 %all-to-all-start = ((f32[4,1,384]{2,1,0:T(1,128)}), f32[4,1,384]{2,1,0:T(1,128)S(1)}, u32[]{:S(2)}, u32[]{:S(2)}) async-start(f32[4,1,384]{2,1,0:T(1,128)} %broadcast_in_dim.6), calls=%async_computation | async-start | bytes 12288 | tf_op jit(solution)/shard_map/all_to_all | solution.py:13
  13.5 263.6 %all-gather.2.cloned.1.call-start = ((), (), s32[]{:S(2)}) async-start(), calls=%async_computation.5 | async-start | bytes 5898240 | tf_op jit(solution)/shard_map/all_gather | solution.py:105
  15.3 3.8 copy-start.2
  224.1 53.0 %copy-start.6 = (bf16[1,2048,256]{2,1,0:T(8,128)(2,1)S(1)}, bf16[1,2048,256]{2,1,0:T(8,128)(2,1)}, u32[]{:S(2)}) copy-start(bf16[1,2048,256]{2,1,0:T(8,128)(2,1)} %param.15) | copy-start | bytes 3145732
  224.2 56.8 %copy-start.7 = (bf16[1,2048,256]{2,1,0:T(8,128)(2,1)S(1)}, bf16[1,2048,256]{2,1,0:T(8,128)(2,1)}, u32[]{:S(2)}) copy-start(bf16[1,2048,256]{2,1,0:T(8,128)(2,1)} %param.16) | copy-start | bytes 3145732
  277.1 3.9 copy-start.5
  331.2 23.4 %copy-start.3 = (f32[384,2]{0,1:T(2,128)S(1)}, f32[384,2]{0,1:T(2,128)}, u32[]{:S(2)}) copy-start(f32[384,2]{0,1:T(2,128)} %param.13) | copy-start | bytes 9220
  331.2 23.4 %copy-start.4 = (f32[384]{0:T(512)S(1)}, f32[384]{0:T(512)}, u32[]{:S(2)}) copy-start(f32[384]{0:T(512)} %param.12) | copy-start | bytes 4612
  331.2 137.9 %all-to-all-start.4 = ((bf16[32,2,1,1,18,512]{5,1,4,3,2,0:T(2,128)(2,1)}), bf16[32,2,1,1,18,512]{5,1,4,3,2,0:T(2,128)(2,1)}, u32[]{:S(2)}, u32[]{:S(2)}) async-start(bf16[32,2,1,1,18,512]{5,1,4,3,2,0:T(2,128)(2,1)} %copy.42), calls=%async_computation.4 | async-start | bytes 2359296 | tf_op jit(solution)/shard_map/all_to_all | solution.py:44
  472.0 2.1 copy-start.1
Sparse Core Ops, SparseCore 0:
  224.3 52.7 all-gather.1
where the time goes:
time: 483 us; the launch traced here: 482 us
  blocking collectives  237 us (49%)
  waiting for transfers between devices  167 us (35%)
  starting transfers between devices  28.5 us (6%)
  local copies, waits for them, and re-layouts  17.8 us (4%)
  matrix products  13.9 us (3%)
  between operations  13.6 us (3%)
    all_to_all x1, blocking collectives, body(): lax.all_to_all(buffer, EP, split_axis=0, concat_axis=0, tiled=True)  200 us
    all_to_all x1, waiting for transfers between devices, moved_by_axis(): lax.all_to_all(blocks, axes[k], split_axis=k, concat_axis=k, tiled=True)  115 us
    all_gather x1, waiting for transfers between devices, body(): lax.all_gather(lax.all_to_all(buffer, EP, split_axis=0, concat_axis=0, ti...  52.9 us
    all_to_all x1, blocking collectives, copy_for_each(): lax.all_to_all(jnp.broadcast_to(array[None], (length, *array.shape)), axi...  31.1 us
    all_to_all x1, starting transfers between devices, moved_by_axis(): lax.all_to_all(blocks, axes[k], split_axis=k, concat_axis=k, tiled=True)  23.3 us
  transfers between devices with their start and end apart: 3, of which 2 were waited for; matrix products, arithmetic and copies ran while one was open for 1% of the time, Pallas kernels for 0%

commit v1 on v0

--- a/solution.py
+++ b/solution.py
@@ -3,6 +3,7 @@
 from jax import lax
 from jax.sharding import Mesh
 from jax.sharding import PartitionSpec as P
+from jax.lax import all_to_all, psum
 
 EP = ("ep_0", "ep_1")
 GRP_EP = ("grp", "ep_0", "ep_1")
@@ -102,12 +103,16 @@
     normed = (values * inv_rms[:, None] * gain_piece[None, :]).astype(jnp.bfloat16)
     buffer = jnp.dot(dispatch, normed, preferred_element_type=jnp.float32).astype(jnp.bfloat16)
     buffer = buffer.reshape(ep_count, exp_local, capacity, piece_width)
-    piece = lax.all_gather(
-        lax.all_to_all(buffer, EP, split_axis=0, concat_axis=0, tiled=True),
-        "tp",
-        axis=3,
-        tiled=True,
-    )
+
+    def _change_pipes(local_x, dim_k):
+        num_devices = psum(1, "tp")
+        by_place = []
+        for m in [*range(local_x.ndim)]:
+            by_place.append(num_devices if m == dim_k else 1)
+        local_out = jnp.tile(local_x, by_place)
+        return all_to_all(local_out, "tp", concat_axis=dim_k, split_axis=dim_k, tiled=True)
+
+    piece = _change_pipes(lax.all_to_all(buffer, EP, split_axis=0, concat_axis=0, tiled=True), 3)
     gate_next = jnp.einsum("sxcd,xdf->sxcf", piece, w_gate, preferred_element_type=jnp.float32)
     up_next = jnp.einsum("sxcd,xdf->sxcf", piece, w_up, preferred_element_type=jnp.float32)
     results = finish_rows(gate_next, up_next, w_down)

time: 483 us -> 508 us (1.052)
  blocking collectives: 237 us -> 295 us
  waiting for transfers between devices: 167 us -> 115 us
  local copies, waits for them, and re-layouts: 17.8 us -> 66.3 us
  starting transfers between devices: 28.5 us -> 12.3 us
  between operations: 13.6 us -> 0.21 us
    all_to_all x0 -> x1, blocking collectives: none -> 58.6 us  [_change_pipes(): all_to_all(local_out, 'tp', concat_axis=dim_k, split_axis=dim_k, tiled=True)]
    all_gather x1 -> x0, waiting for transfers between devices: 52.9 us -> none  [body(): lax.all_gather(lax.all_to_all(buffer, EP, split_axis=0, concat_axis=0, ti...]
    unnamed x17 -> x19, local copies, waits for them, and re-layouts: 0.85 us -> 23.1 us
    all_to_all x1, starting transfers between devices: 23.3 us -> 7.16 us  [moved_by_axis(): lax.all_to_all(blocks, axes[k], split_axis=k, concat_axis=k, tiled=True)]
    another operation x1 -> x3, local copies, waits for them, and re-layouts: 2.9 us -> 16.7 us  [the longest x2 13.7 us: _change_pipes(): local_out = jnp.tile(local_x, by_place)]
    all_to_all x1, local copies, waits for them, and re-layouts: 1.42 us -> 13.9 us  [_change_pipes(): all_to_all(local_out, 'tp', concat_axis=dim_k, split_axis=dim_k, tiled=True)]
  transfers between devices with their start and end apart: 3 -> 2, of which waited for: 2 -> 1; matrix products, arithmetic and copies ran while one was open for 1% -> 1% of each run, Pallas kernels for 0% -> 0%
where the time goes in v1:
time: 508 us; the launch traced here: 507 us
  blocking collectives  295 us (58%)
  waiting for transfers between devices  115 us (23%)
  local copies, waits for them, and re-layouts  66.3 us (13%)
  matrix products  13.9 us (3%)
  starting transfers between devices  12.3 us (2%)
    all_to_all x1, blocking collectives, body(): lax.all_to_all(buffer, EP, split_axis=0, concat_axis=0, tiled=True)  200 us
    all_to_all x1, waiting for transfers between devices, moved_by_axis(): lax.all_to_all(blocks, axes[k], split_axis=k, concat_axis=k, tiled=True)  115 us
    all_to_all x1, blocking collectives, _change_pipes(): all_to_all(local_out, 'tp', concat_axis=dim_k, split_axis=dim_k, tiled=True)  58.6 us
    all_to_all x1, blocking collectives, copy_for_each(): lax.all_to_all(jnp.broadcast_to(array[None], (length, *array.shape)), axi...  28.5 us
    unnamed x19, local copies, waits for them, and re-layouts  23.1 us
    all_to_all x1, local copies, waits for them, and re-layouts, _change_pipes(): all_to_all(local_out, 'tp', concat_axis=dim_k, split_axis=dim_k, tiled=True)  13.9 us
    another operation x2, local copies, waits for them, and re-layouts, _change_pipes(): local_out = jnp.tile(local_x, by_place)  13.7 us
  transfers between devices with their start and end apart: 2, of which 1 were waited for; matrix products, arithmetic and copies ran while one was open for 1% of the time, Pallas kernels for 0%

profile of v1, /device:TPU:33, one launch (start us, length us, event | category | flops | bytes accessed | tf_op | source)
XLA Modules:
  0.0 506.6 jit_solution(6576323291717632172)
XLA Ops:
  0.0 1.2 fusion.35
  1.2 0.6 broadcast_in_dim.6
  1.8 5.1 %all-to-all-start = ((f32[4,1,384]{2,1,0:T(1,128)}), f32[4,1,384]{2,1,0:T(1,128)S(1)}, u32[]{:S(2)}, u32[]{:S(2)}) async-start(f32[4,1,384]{2,1,0:T(1,128)} %broadcast_in_dim.6), calls=%async_computation | async-start | bytes 12288 | tf_op jit(solution)/shard_map/all_to_all | solution.py:14
  7.0 0.9 copy.37
  7.8 0.7 broadcast_multiply_fusion
  9.0 1.8 reduce-window.6
  11.8 0.8 dynamic_slice.3
  12.6 1.9 convolution_convert_fusion
  14.5 2.2 reshape.73
  16.7 199.6 %all_to_all.31 = bf16[64,1,18,512]{3,2,1,0:T(8,128)(2,1)} all-to-all(bf16[64,1,18,512]{3,2,1,0:T(8,128)(2,1)S(1)} %bitcast.93), channel_id=1, replica_groups=mesh['grp'=2,'ep_0'=32,'ep_1'=2,'tp'=4] {'ep_0','ep_1'}, dimensions={0} | all-to-all | bytes 2359296 | tf_op jit(solution)/shard_map/all_to_all | solution.py:115
  216.3 5.7 %copy.41 = bf16[64,18,512]{0,1,2:T(8,128)(2,1)} copy(bf16[64,18,512]{2,1,0:T(8,128)(2,1)} %bitcast.94) | data formatting | bytes 2359296 | tf_op jit(solution)/shard_map/tile | solution.py:112
  222.0 8.1 %tile.12 = bf16[64,18,4,512]{0,1,3,2:T(8,128)(2,1)} broadcast(bf16[64,18,512]{0,1,2:T(8,128)(2,1)} %copy.41), dimensions={0,1,3} | broadcast | bytes 5898240 | tf_op jit(solution)/shard_map/tile | solution.py:112
  230.0 10.1 %reshape.87 = bf16[4,2,294912]{2,1,0:T(2,128)(2,1)} reshape(bf16[2048,1,18,64]{3,2,1,0:T(8,128)(2,1)} %bitcast.91) | data formatting | bytes 9437184
  240.2 58.6 %all_to_all.32 = bf16[4,2,294912]{2,1,0:T(2,128)(2,1)} all-to-all(bf16[4,2,294912]{2,1,0:T(2,128)(2,1)} %reshape.87), channel_id=1, replica_groups=mesh['grp'=2,'ep_0'=32,'ep_1'=2,'tp'=4] {'tp'}, dimensions={0} | all-to-all | bytes 9437184 | tf_op jit(solution)/shard_map/all_to_all | solution.py:113
  298.8 11.9 %reshape.88 = bf16[2048,1,18,64]{3,2,1,0:T(8,128)(2,1)} reshape(bf16[4,2,294912]{2,1,0:T(2,128)(2,1)} %all_to_all.32) | data formatting | bytes 9437184
  310.7 13.9 %copy.42 = bf16[64,1,18,2048]{3,0,2,1:T(8,128)(2,1)} copy(bf16[64,1,18,2048]{0,2,1,3:T(8,128)(2,1)} %bitcast.90) | data formatting | bytes 9437184 | tf_op jit(solution)/shard_map/all_to_all | solution.py:113
  324.6 3.9 fusion.9
  328.7 1.5 fusion.25
  330.2 0.3 broadcast_in_dim.8
  330.5 28.5 %all_to_all.33 = bf16[4,64,1,18,256]{4,1,3,2,0:T(8,128)(2,1)S(1)} all-to-all(bf16[4,64,1,18,256]{4,1,3,2,0:T(8,128)(2,1)S(1)} %broadcast_in_dim.8), channel_id=1, replica_groups=mesh['grp'=2,'ep_0'=32,'ep_1'=2,'tp'=4] {'tp'}, dimensions={0} | all-to-all | bytes 4718592 | tf_op jit(solution)/shard_map/all_to_all | solution.py:14
  359.0 2.0 copy.43
  361.1 2.9 reshape.77
  364.0 3.0 fusion.8
  367.0 0.5 reshape_reshape.3
  367.8 8.4 %all_to_all.34 = bf16[32,2,1,1,18,512]{5,0,4,3,2,1:T(8,128)(2,1)S(1)} all-to-all(bf16[32,2,1,1,18,512]{5,0,4,3,2,1:T(8,128)(2,1)S(1)} %copy.44), channel_id=1, replica_groups=mesh['grp'=2,'ep_0'=32,'ep_1'=2,'tp'=4] {'ep_1'}, dimensions={1} | all-to-all | bytes 2359296 | tf_op jit(solution)/shard_map/all_to_all | solution.py:45
  376.2 2.3 copy.45
  378.5 7.2 %all-to-all-start.5 = ((bf16[32,2,1,1,18,512]{5,1,4,3,2,0:T(2,128)(2,1)}), bf16[32,2,1,1,18,512]{5,1,4,3,2,0:T(2,128)(2,1)}, u32[]{:S(2)}, u32[]{:S(2)}) async-start(bf16[32,2,1,1,18,512]{5,1,4,3,2,0:T(2,128)(2,1)} %copy.45), calls=%async_computation.5 | async-start | bytes 2359296 | tf_op jit(solution)/shard_map/all_to_all | solution.py:45
  385.7 114.5 %all-to-all-done.5 = bf16[32,2,1,1,18,512]{5,1,4,3,2,0:T(2,128)(2,1)} async-done(((bf16[32,2,1,1,18,512]{5,1,4,3,2,0:T(2,128)(2,1)}), bf16[32,2,1,1,18,512]{5,1,4,3,2,0:T(2,128)(2,1)}, u32[]{:S(2)}, u32[]{:S(2)}) %all-to-all-start.5) | async-done | bytes 1179680 | tf_op jit(solution)/shard_map/all_to_all | solution.py:45
  500.2 1.6 copy.46
  501.8 1.2 reshape_reshape_reshape.3
  503.0 2.1 fusion.23
  505.1 1.5 fusion.24
  (33 shorter events, 1.9 us)
Async XLA Ops:
  0.0 364.0 %copy-start = (bf16[1,1024,512]{2,1,0:T(8,128)(2,1)S(1)}, bf16[1,1024,512]{2,1,0:T(8,128)(2,1)}, u32[]{:S(2)}) copy-start(bf16[1,1024,512]{2,1,0:T(8,128)(2,1)} %param.17) | copy-start | bytes 3145732
  1.8 10.7 %all-to-all-start = ((f32[4,1,384]{2,1,0:T(1,128)}), f32[4,1,384]{2,1,0:T(1,128)S(1)}, u32[]{:S(2)}, u32[]{:S(2)}) async-start(f32[4,1,384]{2,1,0:T(1,128)} %broadcast_in_dim.6), calls=%async_computation | async-start | bytes 12288 | tf_op jit(solution)/shard_map/all_to_all | solution.py:14
  7.0 5.6 %copy-start.3 = (bf16[384,512]{1,0:T(8,128)(2,1)S(1)}, bf16[384,512]{1,0:T(8,128)(2,1)}, u32[]{:S(2)}) copy-start(bf16[384,512]{1,0:T(8,128)(2,1)} %param.9) | copy-start | bytes 1179652
  310.7 13.9 %copy-start.6 = (bf16[1,2048,256]{2,1,0:T(8,128)(2,1)S(1)}, bf16[1,2048,256]{2,1,0:T(8,128)(2,1)}, u32[]{:S(2)}) copy-start(bf16[1,2048,256]{2,1,0:T(8,128)(2,1)} %param.15) | copy-start | bytes 3145732
  324.6 3.9 copy-start.1
  324.6 4.1 copy-start.7
  378.5 7.2 %copy-start.4 = (f32[384,2]{0,1:T(2,128)S(1)}, f32[384,2]{0,1:T(2,128)}, u32[]{:S(2)}) copy-start(f32[384,2]{0,1:T(2,128)} %param.13) | copy-start | bytes 9220
  378.5 7.2 %copy-start.5 = (f32[384]{0:T(512)S(1)}, f32[384]{0:T(512)}, u32[]{:S(2)}) copy-start(f32[384]{0:T(512)} %param.12) | copy-start | bytes 4612
  378.5 121.8 %all-to-all-start.5 = ((bf16[32,2,1,1,18,512]{5,1,4,3,2,0:T(2,128)(2,1)}), bf16[32,2,1,1,18,512]{5,1,4,3,2,0:T(2,128)(2,1)}, u32[]{:S(2)}, u32[]{:S(2)}) async-start(bf16[32,2,1,1,18,512]{5,1,4,3,2,0:T(2,128)(2,1)} %copy.45), calls=%async_computation.5 | async-start | bytes 2359296 | tf_op jit(solution)/shard_map/all_to_all | solution.py:45
  503.0 2.1 copy-start.2
